TPU v7x, 256 devices: a 4x2x16 block of a 4x16x16 slice. The times are simulated.
256 devices in a mesh: grp: 2 (over y), sp: 16 (over z), tp: 8 (over x, core).
Axes of the slice: x: 4, y: 2, z: 16, core: 2. Of those that a mesh axis runs over, the one named last changes fastest.
The devices are a block of a 4x16x16 slice.
Arguments:
- queries: bfloat16 [16384, 2048], P(('grp', 'sp'), 'tp'), parts along dimension 0, may hold values from -6 to 6
- key_vectors: bfloat16 [16384, 2048], P(('grp', 'sp'), 'tp'), parts along dimension 0, may hold values from -6 to 6
- value_vectors: bfloat16 [16384, 2048], P(('grp', 'sp'), 'tp'), parts along dimension 0, may hold values from -6 to 6
- forget_sums: float32 [16384, 16], P(('grp', 'sp'), 'tp'), parts along dimension 0, may hold values from -8192 to 0, as said below
- residual: bfloat16 [16384, 2048], P(('grp', 'sp'), 'tp'), parts along dimension 0, may hold values from -20 to 20
- query_gain: float32 [128], replicated, may hold values from 0.5 to 5
- key_gain: float32 [128], replicated, may hold values from 0.5 to 5
- out_weight: bfloat16 [2048, 2048], P(None, 'tp'), may hold values from -0.125 to 0.125
- norm_gain: float32 [2048], replicated, may hold values from 0.1 to 1.9
- gate_weight: bfloat16 [2048, 5504], P('sp', 'tp'), may hold values from -0.125 to 0.125
- up_weight: bfloat16 [2048, 5504], P('sp', 'tp'), may hold values from -0.125 to 0.125
- down_weight: bfloat16 [2048, 5504], P('sp', 'tp'), may hold values from -0.078125 to 0.078125
Outputs:
- layer_output: bfloat16 [16384, 2048], P(('grp', 'sp'), 'tp'), parts along dimension 0
There are 2 independent parts, one for each index of `grp`. A program takes and returns all parts, laid end to end along the dimension named above; an argument that names none is the same for every part. Nothing has to cross between parts.
Inputs may be any that keep to these rules, and one draw needn't show every extreme that they name: `forget_sums`: along positions each head's values never rise.
All inputs are finite; a program needn't handle non-finite values.
Results may differ from a plain program's by a relative error of at most 0.011.
Values may be sent and summed in bfloat16 or wider, within the bound.
A program may use at most 128 MiB of HBM per device.

v0:
```python
import math

import jax
import jax.numpy as jnp
from jax import lax
from jax.sharding import PartitionSpec as P

HEAD = 128


eps = 1e-06


def in_one_piece(arrays, axis, dim, along):
    both = jnp.concatenate(arrays, axis=along)
    filled, at, finished = (lax.all_gather(both, axis, axis=dim, tiled=True), 0, [])
    for a in arrays:
        finished.append(lax.slice_in_dim(filled, at, at + a.shape[along], axis=along))
        at += a.shape[along]
    return tuple(finished)


def copy_for_each(shard, axis):
    copies = jnp.broadcast_to(shard, (lax.axis_size(axis), *shard.shape))
    return lax.all_to_all(copies, axis, split_axis=0, concat_axis=0, tiled=True)


def in_order(pieces, dim):
    dims = list(pieces.shape[1:])
    dims[dim] *= pieces.shape[0]
    return jnp.moveaxis(pieces, 0, dim).reshape(dims)


def gather_directly(shard, axis, dim):
    pieces = copy_for_each(shard, axis)
    return in_order(pieces, dim)


def cut_along(shard, dim, length):
    dims = shard.shape
    pieces = shard.reshape(*dims[:dim], length, dims[dim] // length, *dims[dim + 1 :])
    return jnp.moveaxis(pieces, dim, 0)


def summed_on_arrival(shard, axis, dim):
    length = lax.axis_size(axis)
    pieces = lax.all_to_all(cut_along(shard, dim, length), axis, 0, 0, tiled=True)
    return jnp.sum(pieces.astype(jnp.float32), axis=0)


def head_norm(rows_in, gain):
    count = rows_in.shape[0]
    split = rows_in.reshape(count, -1, HEAD).astype(jnp.float32)
    factor = lax.rsqrt(jnp.mean(split * split, axis=2, keepdims=True) + eps)
    return (split * factor * gain).astype(jnp.bfloat16)


def local(
    queries,
    key_vectors,
    value_vectors,
    forget_sums,
    residual,
    query_gain,
    key_gain,
    out_weight,
    norm_gain,
    gate_weight,
    up_weight,
    down_weight,
):
    whole_gate, whole_up, whole_down = in_one_piece(
        (gate_weight, up_weight, down_weight), "sp", 0, 1
    )
    local_rows = queries.shape[0]
    query_norm = head_norm(queries, query_gain)
    heads_here = query_norm.shape[1]
    key_norm = head_norm(key_vectors, key_gain).reshape(local_rows, heads_here * HEAD)
    offset = lax.axis_index("sp") * local_rows
    query_pos = offset + lax.iota(jnp.int32, local_rows)
    last_query = offset + local_rows - 1
    query_bias = forget_sums.T
    key_bias_all = gather_directly(forget_sums, "sp", 0).T
    factor_scale = 1.0 / math.sqrt(HEAD)
    initial = (
        jnp.full((heads_here, local_rows), -1e30, jnp.float32),
        jnp.zeros((heads_here, local_rows), jnp.float32),
        jnp.zeros((local_rows, heads_here, HEAD), jnp.float32),
    )
    keys_in, values_in = in_one_piece((key_norm, value_vectors), "sp", 0, 1)
    count = keys_in.shape[0]
    block = math.gcd(count, 2048)
    turns = count // block
    key_blocks = keys_in.reshape(turns, block, heads_here, HEAD)
    value_blocks = values_in.reshape(turns, block, heads_here, HEAD)
    starts = block * lax.iota(jnp.int32, turns)

    def visit(state, item):
        key_block, value_block, first = item

        def live(inner):
            running_max, running_sum, weighted = inner
            scores = (
                jnp.einsum(
                    "qhd,khd->hqk", query_norm, key_block, preferred_element_type=jnp.float32
                )
                * factor_scale
            )
            key_bias = lax.dynamic_slice_in_dim(key_bias_all, first, block, 1)
            scores = scores + query_bias[:, :, None] - key_bias[:, None, :]
            key_pos = first + lax.iota(jnp.int32, block)
            allowed = key_pos[None, :] <= query_pos[:, None]
            scores = jnp.where(allowed[None], scores, -1e30)
            new_max = jnp.maximum(running_max, jnp.max(scores, axis=2))
            raised = jnp.where(allowed[None], jnp.exp(scores - new_max[:, :, None]), 0.0)
            shrink = jnp.exp(running_max - new_max)
            running_sum = shrink * running_sum + jnp.sum(raised, axis=2)
            update = jnp.einsum(
                "hqk,khd->qhd",
                raised.astype(jnp.bfloat16),
                value_block,
                preferred_element_type=jnp.float32,
            )
            weighted = weighted * shrink.T[:, :, None] + update
            return (new_max, running_sum, weighted)

        def skip(inner):
            return inner

        return (lax.cond(first <= last_query, live, skip, state), None)

    result, _ = lax.scan(visit, initial, (key_blocks, value_blocks, starts))
    running_max, running_sum, weighted = result
    attended = (
        (weighted / running_sum.T[:, :, None])
        .astype(jnp.bfloat16)
        .reshape(local_rows, heads_here * HEAD)
    )
    projected = jnp.dot(
        gather_directly(attended, "tp", 1), out_weight, preferred_element_type=jnp.float32
    )
    middle = (residual.astype(jnp.float32) + projected).astype(jnp.bfloat16)
    whole_rows = gather_directly(middle, "tp", 1).astype(jnp.float32)
    normed = (
        whole_rows
        * lax.rsqrt(jnp.mean(whole_rows * whole_rows, axis=1, keepdims=True) + eps)
        * norm_gain
    ).astype(jnp.bfloat16)
    gate = jnp.dot(normed, whole_gate, preferred_element_type=jnp.float32)
    upward = jnp.dot(normed, whole_up, preferred_element_type=jnp.float32)
    hidden = (jax.nn.silu(gate) * upward).astype(jnp.bfloat16)
    terms = lax.dot_general(
        hidden, whole_down, (((1,), (1,)), ((), ())), preferred_element_type=jnp.float32
    )
    summed = summed_on_arrival(terms.astype(jnp.bfloat16), "tp", 1)
    return (middle.astype(jnp.float32) + summed).astype(jnp.bfloat16)


def solution(mesh):
    placed = (
        P(("grp", "sp"), "tp"),
        P(("grp", "sp"), "tp"),
        P(("grp", "sp"), "tp"),
        P(("grp", "sp"), "tp"),
        P(("grp", "sp"), "tp"),
        P(),
        P(),
        P(None, "tp"),
        P(),
        P("sp", "tp"),
        P("sp", "tp"),
        P("sp", "tp"),
    )
    return jax.shard_map(
        local, mesh=mesh, in_specs=placed, out_specs=P(("grp", "sp"), "tp"), check_vma=False
    )
```

profile of v0, /device:TPU:1568, one launch (start us, length us, event | category | flops | bytes accessed | tf_op | source)
XLA Modules:
  0.0 327.2 jit_solution(17241046151288033677)
XLA Ops:
  6.7 1.1 convert_multiply_fusion.3
  8.1 0.6 reduce_sum.47
  8.7 0.7 broadcast_bitcast_fusion
  9.4 0.6 mul.110
  10.0 1.0 fusion.43
  11.0 0.9 pad_maximum_fusion.1
  12.1 0.9 pad_maximum_fusion
  13.0 0.6 broadcast_in_dim.61
  13.6 8.5 %all-to-all-start = ((f32[16,512,2]{1,2,0:T(2,128)}), f32[16,512,2]{1,2,0:T(2,128)S(1)}, u32[]{:S(2)}, u32[]{:S(2)}) async-start(f32[16,512,2]{1,2,0:T(2,128)} %broadcast_in_dim.61), calls=%async_computation | async-start | bytes 131072 | tf_op jit(solution)/shard_map/all_to_all | solution.py:25
  22.7 92.2 %all-gather.3.cloned.1.call-done = bf16[8192,512]{1,0:T(8,128)(2,1)} async-done(((bf16[512,512]{1,0:T(8,128)(2,1)}), bf16[8192,512]{1,0:T(8,128)(2,1)}) %all-gather.3.cloned.1.call-update) | async-done | bytes 8388624 | tf_op jit(solution)/shard_map/all_gather | solution.py:16
  114.9 5.7 %fusion.48 = (bf16[8192,256]{1,0:T(8,128)(2,1)}, bf16[8192,256]{1,0:T(8,128)(2,1)}) fusion(bf16[8192,512]{1,0:T(8,128)(2,1)} %all-gather.3.cloned.1.call-done), kind=kLoop, calls=%fused_computation.63 | loop fusion | bytes 16777216 | tf_op jit(solution)/shard_map/slice | solution.py:18
  120.6 6.9 %reshape.93 = bf16[4,2048,2,128]{3,2,1,0:T(2,128)(2,1)} reshape(bf16[8192,256]{1,0:T(8,128)(2,1)} %get-tuple-element.277) | data formatting | bytes 8388608 | tf_op jit(solution)/shard_map/reshape | solution.py:94
  127.5 4.7 %copy.46 = bf16[4,2048,2,128]{3,1,2,0:T(8,128)(2,1)} copy(bf16[4,2048,2,128]{3,2,1,0:T(2,128)(2,1)} %reshape.93) | data formatting | bytes 8388608
  132.2 7.0 %reshape.95 = bf16[4,2048,2,128]{3,2,1,0:T(2,128)(2,1)} reshape(bf16[8192,256]{1,0:T(8,128)(2,1)} %get-tuple-element.276) | data formatting | bytes 8388608 | tf_op jit(solution)/shard_map/reshape | solution.py:95
  139.2 4.7 %copy.48 = bf16[4,2048,2,128]{3,1,2,0:T(8,128)(2,1)} copy(bf16[4,2048,2,128]{3,2,1,0:T(2,128)(2,1)} %reshape.95) | data formatting | bytes 8388608
  144.0 68.7 %while.15 = (s32[]{:T(128)}, f32[2,512]{1,0:T(2,128)S(1)}, f32[2,512]{1,0:T(2,128)S(1)}, f32[512,2,128]{2,0,1:T(8,128)S(1)}, s32[4]{0:T(128)S(1)}, /*index=5*/s3...) while((s32[]{:T(128)}, f32[2,512]{1,0:T(2,128)S(1)}, ...), condition=%wide.region_7.8_spmd.clone, body=%wide.region_2.7_spmd.clone.sunk | while | flops 1114904064 | bytes 32953692 | solution.py:132
  145.2 15.9 %conditional.3 = ((f32[2,512]{1,0:T(2,128)S(1)}, f32[2,512]{1,0:T(2,128)S(1)}, f32[512,2,128]{2,0,1:T(8,128)S(1)})) conditional(s32[]{:T(128)} %convert_element_type.116, (f32[2,512]{1,0:T(2,128)S(1)}, f32[2,512]{1,0:T(2,128)S(1)}, f32[512,2,128]{2,0,1:T(8,128)S(1)}) %tuple.43, (s32[]{:T(128)}, s32[]{:T(128)}, bf16[4,2048,2,128]{3,1,2,0:T(8,128)(2,1)}, ...), branch_computations={%region_3.3_spmd, %region_4.6_spmd} | conditional | flops 1114904064 | bytes 32951374 | solution.py:130
  147.3 0.7 iota_add_fusion
  147.9 0.8 broadcast_compare_fusion
  148.7 4.0 %fusion.4 = (f32[2,512]{1,0:T(2,128)S(1)}, f32[2,2048,512]{2,1,0:T(8,128)S(1)}) fusion(f32[2,2048]{1,0:T(2,128)S(1)} %constant_dynamic-slice_fusion, f32[2,512]{1,0:T(2,128)S(1)} %get-tuple-element.142, pred[512,2048]{0,1:T(8,128)(4,1)S(1)} %broadcast_compare_fusion, bf16[512,2,128]{2,0,1:T(8,128)(2,1)S(1)} %get-tuple-element.141, ...), kind=kOutput, calls=%fused_computation.5 | convolution fusion | flops 547355648 | bytes 10772992 | tf_op jit(solution)/shard_map/while/body/eval_jaxpr/cond/branch_1_fun/qhd,khd->hqk/dot_general | solution.py:104
  152.7 5.5 %fusion.11 = f32[512,2,128]{2,0,1:T(8,128)S(1)} fusion(f32[2,2048,512]{2,1,0:T(8,128)S(1)} %get-tuple-element.275, f32[2,512]{1,0:T(2,128)S(1)} %get-tuple-element.360, f32[2,2048]{1,0:T(2,128)S(1)} %constant_dynamic-slice_fusion, f32[2,512]{1,0:T(2,128)S(1)} %get-tuple-element.142, pred[512,2048]{0,1:T(8,128)(4,1)S(1)} %broadcast_compare_fusion, ...), kind=kOutput, calls=%fused_computation.10 | convolution fusion | flops 551813120 | bytes 11563520 | tf_op jit(solution)/shard_map/while/body/eval_jaxpr/cond/branch_1_fun/hqk,khd->qhd/dot_general | solution.py:118
  158.2 2.9 fusion.3
  162.4 15.9 %conditional.3 = ((f32[2,512]{1,0:T(2,128)S(1)}, f32[2,512]{1,0:T(2,128)S(1)}, f32[512,2,128]{2,0,1:T(8,128)S(1)})) conditional(s32[]{:T(128)} %convert_element_type.116, (f32[2,512]{1,0:T(2,128)S(1)}, f32[2,512]{1,0:T(2,128)S(1)}, f32[512,2,128]{2,0,1:T(8,128)S(1)}) %tuple.43, (s32[]{:T(128)}, s32[]{:T(128)}, bf16[4,2048,2,128]{3,1,2,0:T(8,128)(2,1)}, ...), branch_computations={%region_3.3_spmd, %region_4.6_spmd} | conditional | flops 1114904064 | bytes 32951374 | solution.py:130
  164.4 0.7 iota_add_fusion
  165.1 0.8 broadcast_compare_fusion
  165.9 4.0 %fusion.4 = (f32[2,512]{1,0:T(2,128)S(1)}, f32[2,2048,512]{2,1,0:T(8,128)S(1)}) fusion(f32[2,2048]{1,0:T(2,128)S(1)} %constant_dynamic-slice_fusion, f32[2,512]{1,0:T(2,128)S(1)} %get-tuple-element.142, pred[512,2048]{0,1:T(8,128)(4,1)S(1)} %broadcast_compare_fusion, bf16[512,2,128]{2,0,1:T(8,128)(2,1)S(1)} %get-tuple-element.141, ...), kind=kOutput, calls=%fused_computation.5 | convolution fusion | flops 547355648 | bytes 10772992 | tf_op jit(solution)/shard_map/while/body/eval_jaxpr/cond/branch_1_fun/qhd,khd->hqk/dot_general | solution.py:104
  169.9 5.5 %fusion.11 = f32[512,2,128]{2,0,1:T(8,128)S(1)} fusion(f32[2,2048,512]{2,1,0:T(8,128)S(1)} %get-tuple-element.275, f32[2,512]{1,0:T(2,128)S(1)} %get-tuple-element.360, f32[2,2048]{1,0:T(2,128)S(1)} %constant_dynamic-slice_fusion, f32[2,512]{1,0:T(2,128)S(1)} %get-tuple-element.142, pred[512,2048]{0,1:T(8,128)(4,1)S(1)} %broadcast_compare_fusion, ...), kind=kOutput, calls=%fused_computation.10 | convolution fusion | flops 551813120 | bytes 11563520 | tf_op jit(solution)/shard_map/while/body/eval_jaxpr/cond/branch_1_fun/hqk,khd->qhd/dot_general | solution.py:118
  175.4 2.9 fusion.3
  179.6 15.9 %conditional.3 = ((f32[2,512]{1,0:T(2,128)S(1)}, f32[2,512]{1,0:T(2,128)S(1)}, f32[512,2,128]{2,0,1:T(8,128)S(1)})) conditional(s32[]{:T(128)} %convert_element_type.116, (f32[2,512]{1,0:T(2,128)S(1)}, f32[2,512]{1,0:T(2,128)S(1)}, f32[512,2,128]{2,0,1:T(8,128)S(1)}) %tuple.43, (s32[]{:T(128)}, s32[]{:T(128)}, bf16[4,2048,2,128]{3,1,2,0:T(8,128)(2,1)}, ...), branch_computations={%region_3.3_spmd, %region_4.6_spmd} | conditional | flops 1114904064 | bytes 32951374 | solution.py:130
  181.6 0.7 iota_add_fusion
  182.3 0.8 broadcast_compare_fusion
  183.1 4.0 %fusion.4 = (f32[2,512]{1,0:T(2,128)S(1)}, f32[2,2048,512]{2,1,0:T(8,128)S(1)}) fusion(f32[2,2048]{1,0:T(2,128)S(1)} %constant_dynamic-slice_fusion, f32[2,512]{1,0:T(2,128)S(1)} %get-tuple-element.142, pred[512,2048]{0,1:T(8,128)(4,1)S(1)} %broadcast_compare_fusion, bf16[512,2,128]{2,0,1:T(8,128)(2,1)S(1)} %get-tuple-element.141, ...), kind=kOutput, calls=%fused_computation.5 | convolution fusion | flops 547355648 | bytes 10772992 | tf_op jit(solution)/shard_map/while/body/eval_jaxpr/cond/branch_1_fun/qhd,khd->hqk/dot_general | solution.py:104
  187.1 5.5 %fusion.11 = f32[512,2,128]{2,0,1:T(8,128)S(1)} fusion(f32[2,2048,512]{2,1,0:T(8,128)S(1)} %get-tuple-element.275, f32[2,512]{1,0:T(2,128)S(1)} %get-tuple-element.360, f32[2,2048]{1,0:T(2,128)S(1)} %constant_dynamic-slice_fusion, f32[2,512]{1,0:T(2,128)S(1)} %get-tuple-element.142, pred[512,2048]{0,1:T(8,128)(4,1)S(1)} %broadcast_compare_fusion, ...), kind=kOutput, calls=%fused_computation.10 | convolution fusion | flops 551813120 | bytes 11563520 | tf_op jit(solution)/shard_map/while/body/eval_jaxpr/cond/branch_1_fun/hqk,khd->qhd/dot_general | solution.py:118
  192.6 2.9 fusion.3
  196.7 15.9 %conditional.3 = ((f32[2,512]{1,0:T(2,128)S(1)}, f32[2,512]{1,0:T(2,128)S(1)}, f32[512,2,128]{2,0,1:T(8,128)S(1)})) conditional(s32[]{:T(128)} %convert_element_type.116, (f32[2,512]{1,0:T(2,128)S(1)}, f32[2,512]{1,0:T(2,128)S(1)}, f32[512,2,128]{2,0,1:T(8,128)S(1)}) %tuple.43, (s32[]{:T(128)}, s32[]{:T(128)}, bf16[4,2048,2,128]{3,1,2,0:T(8,128)(2,1)}, ...), branch_computations={%region_3.3_spmd, %region_4.6_spmd} | conditional | flops 1114904064 | bytes 32951374 | solution.py:130
  198.8 0.7 iota_add_fusion
  199.4 0.8 broadcast_compare_fusion
  200.2 4.0 %fusion.4 = (f32[2,512]{1,0:T(2,128)S(1)}, f32[2,2048,512]{2,1,0:T(8,128)S(1)}) fusion(f32[2,2048]{1,0:T(2,128)S(1)} %constant_dynamic-slice_fusion, f32[2,512]{1,0:T(2,128)S(1)} %get-tuple-element.142, pred[512,2048]{0,1:T(8,128)(4,1)S(1)} %broadcast_compare_fusion, bf16[512,2,128]{2,0,1:T(8,128)(2,1)S(1)} %get-tuple-element.141, ...), kind=kOutput, calls=%fused_computation.5 | convolution fusion | flops 547355648 | bytes 10772992 | tf_op jit(solution)/shard_map/while/body/eval_jaxpr/cond/branch_1_fun/qhd,khd->hqk/dot_general | solution.py:104
  204.2 5.5 %fusion.11 = f32[512,2,128]{2,0,1:T(8,128)S(1)} fusion(f32[2,2048,512]{2,1,0:T(8,128)S(1)} %get-tuple-element.275, f32[2,512]{1,0:T(2,128)S(1)} %get-tuple-element.360, f32[2,2048]{1,0:T(2,128)S(1)} %constant_dynamic-slice_fusion, f32[2,512]{1,0:T(2,128)S(1)} %get-tuple-element.142, pred[512,2048]{0,1:T(8,128)(4,1)S(1)} %broadcast_compare_fusion, ...), kind=kOutput, calls=%fused_computation.10 | convolution fusion | flops 551813120 | bytes 11563520 | tf_op jit(solution)/shard_map/while/body/eval_jaxpr/cond/branch_1_fun/hqk,khd->qhd/dot_general | solution.py:118
  209.7 2.9 fusion.3
  213.1 31.4 %all_to_all.20 = bf16[8,512,256]{1,2,0:T(8,128)(2,1)S(1)} all-to-all(bf16[8,512,256]{1,2,0:T(8,128)(2,1)S(1)} %broadcast_in_dim.62), channel_id=1, replica_groups=mesh['grp'=2,'sp'=16,'tp'=8] {'tp'}, dimensions={0} | all-to-all | bytes 4194304 | tf_op jit(solution)/shard_map/all_to_all | solution.py:25
  244.5 0.8 fusion.40
  245.6 29.7 %all_to_all.21 = bf16[8,512,256]{1,2,0:T(8,128)(2,1)S(1)} all-to-all(bf16[8,512,256]{1,2,0:T(8,128)(2,1)S(1)} %broadcast_in_dim.63), channel_id=1, replica_groups=mesh['grp'=2,'sp'=16,'tp'=8] {'tp'}, dimensions={0} | all-to-all | bytes 4194304 | tf_op jit(solution)/shard_map/all_to_all | solution.py:25
  276.5 1.3 copy-done.1
  277.8 4.5 %fusion.30 = f32[512,688]{0,1:T(8,128)} fusion(bf16[512,2048]{0,1:T(8,128)(2,1)S(1)} %fusion.26, bf16[2048,2064]{0,1:T(8,128)(2,1)} %all-gather.5.cloned.1.call-done), kind=kOutput, calls=%fused_computation.36 | convolution fusion | flops 1442840576 | bytes 6324224 | tf_op jit(solution)/shard_map/dot_general | solution.py:149
  282.3 7.1 %convolution_convert_fusion = bf16[512,2048]{1,0:T(8,128)(2,1)S(1)} fusion(bf16[2048,2064]{0,1:T(8,128)(2,1)} %all-gather.5.cloned.1.call-done, bf16[512,2048]{0,1:T(8,128)(2,1)} %copy-done.1, f32[512,688]{0,1:T(8,128)} %fusion.30), kind=kOutput, calls=%fused_computation.32 | convolution fusion | flops 2888843264 | bytes 11239424 | tf_op jit(solution)/shard_map/dot_general | solution.py:152
  289.6 29.7 %all_to_all.22 = bf16[8,512,256]{2,1,0:T(8,128)(2,1)S(1)} all-to-all(bf16[8,512,256]{2,1,0:T(8,128)(2,1)S(1)} %bitcast.68), channel_id=1, replica_groups=mesh['grp'=2,'sp'=16,'tp'=8] {'tp'}, dimensions={0} | all-to-all | bytes 4194304 | tf_op jit(solution)/shard_map/all_to_all | solution.py:47
  319.6 0.8 add_convert_fusion
  (76 shorter events, 6.3 us)
Async XLA Ops:
  6.5 238.0 %copy-start = (bf16[2048,256]{1,0:T(8,128)(2,1)S(1)}, bf16[2048,256]{1,0:T(8,128)(2,1)}, u32[]{:S(2)}) copy-start(bf16[2048,256]{1,0:T(8,128)(2,1)} %param.23) | copy-start | bytes 3145732
  6.6 4.5 %copy-start.3 = (bf16[512,256]{1,0:T(8,128)(2,1)S(1)}, bf16[512,256]{1,0:T(8,128)(2,1)}, u32[]{:S(2)}) copy-start(bf16[512,256]{1,0:T(8,128)(2,1)} %param.18) | copy-start | bytes 786436
  6.6 5.5 %copy-start.6 = (bf16[128,688]{0,1:T(8,128)(2,1)S(1)}, bf16[128,688]{0,1:T(8,128)(2,1)}, u32[]{:S(2)}) copy-start(bf16[128,688]{0,1:T(8,128)(2,1)} %param.25) | copy-start | bytes 528388
  6.6 5.5 %copy-start.5 = (bf16[128,688]{0,1:T(8,128)(2,1)S(1)}, bf16[128,688]{0,1:T(8,128)(2,1)}, u32[]{:S(2)}) copy-start(bf16[128,688]{0,1:T(8,128)(2,1)} %param.26) | copy-start | bytes 528388
  6.6 5.5 %copy-start.4 = (bf16[128,688]{0,1:T(8,128)(2,1)S(1)}, bf16[128,688]{0,1:T(8,128)(2,1)}, u32[]{:S(2)}) copy-start(bf16[128,688]{0,1:T(8,128)(2,1)} %param.27) | copy-start | bytes 528388
  6.6 6.4 %copy-start.7 = (f32[512,2]{0,1:T(2,128)S(1)}, f32[512,2]{0,1:T(2,128)}, u32[]{:S(2)}) copy-start(f32[512,2]{0,1:T(2,128)} %param.19) | copy-start | bytes 12292
  6.6 15.5 %copy-start.2 = (bf16[512,256]{1,0:T(8,128)(2,1)S(1)}, bf16[512,256]{1,0:T(8,128)(2,1)}, u32[]{:S(2)}) copy-start(bf16[512,256]{1,0:T(8,128)(2,1)} %param.16) | copy-start | bytes 786436
  6.6 108.3 %all-gather.3.cloned.1.call-start = ((), (), s32[]{:S(2)}) async-start(), calls=%async_computation.4 | async-start | bytes 8912896 | tf_op jit(solution)/shard_map/all_gather | solution.py:16
  7.8 14.6 %copy-start.9 = (f32[128]{0:T(128)S(1)}, f32[128]{0:T(128)}, u32[]{:S(2)}) copy-start(f32[128]{0:T(128)} %param.21) | copy-start | bytes 1540
  11.9 264.5 %all-gather.5.cloned.1.call-start = ((), (), s32[]{:S(2)}) async-start(), calls=%async_computation.5 | async-start | bytes 8982528 | tf_op jit(solution)/shard_map/all_gather | solution.py:16
  13.6 130.3 %all-to-all-start = ((f32[16,512,2]{1,2,0:T(2,128)}), f32[16,512,2]{1,2,0:T(2,128)S(1)}, u32[]{:S(2)}, u32[]{:S(2)}) async-start(f32[16,512,2]{1,2,0:T(2,128)} %broadcast_in_dim.61), calls=%async_computation | async-start | bytes 131072 | tf_op jit(solution)/shard_map/all_to_all | solution.py:25
  212.6 31.9 %copy-start.10 = (bf16[512,256]{1,0:T(8,128)(2,1)S(1)}, bf16[512,256]{1,0:T(8,128)(2,1)}, u32[]{:S(2)}) copy-start(bf16[512,256]{1,0:T(8,128)(2,1)} %param.20) | copy-start | bytes 786436
  245.4 30.5 %copy-start.8 = (f32[2048]{0:T(1024)S(1)}, f32[2048]{0:T(1024)}, u32[]{:S(2)}) copy-start(f32[2048]{0:T(1024)} %param.24) | copy-start | bytes 24580
  276.5 1.4 copy-start.1
Sparse Core Ops, SparseCore 0:
  12.1 102.7 all-gather.2
  116.6 122.4 all-gather.4
where the time goes:
time: 328 us; the launch traced here: 327 us
  waiting for transfers between devices  92.3 us (28%)
  blocking collectives  90.9 us (28%)
  matrix products  50.3 us (15%)
  local copies, waits for them, and re-layouts  36.5 us (11%)
  other arithmetic  24.1 us (7%)
  between operations  13.7 us (4%)
  loops' own time  10.8 us (3%)
  starting transfers between devices  8.61 us (3%)
    all_gather x2, waiting for transfers between devices, in_one_piece(): lax.all_gather(both, axis, axis=dim, tiled=True)  92.2 us
    all_to_all x2, blocking collectives, copy_for_each(): return lax.all_to_all(copies, axis, split_axis=0, concat_axis=0, tiled=True)  61.2 us
    all_to_all x1, blocking collectives, summed_on_arrival(): lax.all_to_all(cut_along(shard, dim, length), axis, 0, 0, tiled=True)  29.7 us
    dot_general x4, matrix products, live(): jnp.einsum('hqk,khd->qhd', raised.astype(jnp.bfloat16), value_block, pref...  22 us
    dot_general x4, matrix products, live(): jnp.einsum('qhd,khd->hqk', query_norm, key_block, preferred_element_type=...  15.9 us
    reduce_sum x4, other arithmetic, live(): running_sum = shrink * running_sum + jnp.sum(raised, axis=2)  11.4 us
    unnamed x26, local copies, waits for them, and re-layouts  11.1 us
    all_to_all x1, starting transfers between devices, copy_for_each(): return lax.all_to_all(copies, axis, split_axis=0, concat_axis=0, tiled=True)  8.48 us
  transfers between devices with their start and end apart: 3, of which 1 were waited for; matrix products, arithmetic and copies ran while one was open for 28% of the time, Pallas kernels for 0%

commit v1 on v0

v1 whole, which is shorter than its diff:
```python
import functools
import math

import jax
import jax.numpy as jnp
from jax import lax
from jax.experimental import pallas as pl
from jax.experimental.pallas import tpu as pltpu
from jax.sharding import PartitionSpec as P

MESH = pl.DeviceIdType.MESH
HEAD = 128
EPS = 1e-06
LOW = -1e30
LOG2E = 1.4426950408889634


def remote(src, dst, send, recv, device):
    return pltpu.make_async_remote_copy(
        src_ref=src, dst_ref=dst, send_sem=send, recv_sem=recv, device_id=device, device_id_type=MESH
    )


def arrived(ref, sem, device):
    remote(ref, ref, sem, sem, device).wait_recv()


def left_over(ref, sem, device):
    remote(ref, ref, sem, sem, device).wait_send()


class Row:
    def __init__(self, t, size):
        self.t = t
        self.left = lax.rem(t + size - 2, size)
        self.right = lax.rem(t + 2, size)
        self.opp = lax.rem(t + size // 2, size)
        self.core = lax.rem(t, 2)

    @staticmethod
    def other(t):
        return t + 1 - 2 * lax.rem(t, 2)


def row_gather(row, buf, send, recv):
    half = buf.shape[1] // 2
    t, left, right, opp = row.t, row.left, row.right, row.opp
    other = Row.other
    to_left, to_right, to_other = {"tp": left}, {"tp": right}, {"tp": other(t)}
    first, second = pl.ds(0, half), pl.ds(half, half)
    sent = []

    def go(ref, at, device):
        copy = remote(ref, ref, send.at[at], recv.at[at], device)
        copy.start()
        sent.append(copy)

    go(buf.at[t], 0, to_right)
    go(buf.at[t], 1, to_left)
    go(buf.at[t], 2, to_other)
    arrived(buf.at[left], recv.at[0], to_left)
    go(buf.at[left, first], 3, to_right)
    go(buf.at[left], 4, to_other)
    arrived(buf.at[right], recv.at[1], to_right)
    go(buf.at[right, second], 5, to_left)
    go(buf.at[right], 6, to_other)
    arrived(buf.at[opp, first], recv.at[3], to_left)
    go(buf.at[opp, first], 7, to_other)
    arrived(buf.at[opp, second], recv.at[5], to_right)
    go(buf.at[opp, second], 8, to_other)
    arrived(buf.at[other(t)], recv.at[2], to_other)
    arrived(buf.at[other(left)], recv.at[4], to_other)
    arrived(buf.at[other(right)], recv.at[6], to_other)
    arrived(buf.at[other(opp), first], recv.at[7], to_other)
    arrived(buf.at[other(opp), second], recv.at[8], to_other)
    for copy in sent:
        copy.wait_send()


def normed(rows, gain):
    square = jnp.mean(rows * rows, axis=-1, keepdims=True)
    return rows * lax.rsqrt(square + EPS) * gain


def attention_kernel(
    n_sp,
    n_tp,
    q_ref,
    k_ref,
    v_ref,
    f_ref,
    res_ref,
    ow_ref,
    qg_ref,
    kg_ref,
    out_ref,
    qbuf,
    kv,
    fbuf,
    kn,
    obuf,
    att,
    mid,
    send_a,
    recv_a,
    send_b,
    recv_b,
    send_c,
    recv_c,
    send_o,
    recv_o,
    send_g,
    recv_g,
    out_sem,
):
    s = lax.axis_index("sp")
    t = lax.axis_index("tp")
    row = Row(t, n_tp)
    other = Row.other
    left, right, opp = row.left, row.right, row.opp
    sub = qbuf.shape[1]
    per = n_sp // 4

    def row_of(head):
        return lax.rem(head, per) * 4 + head // per

    def head_of(r):
        return lax.rem(r, 4) * per + r // 4

    my_head = head_of(s)
    source = my_head // 2

    barrier = pltpu.get_barrier_semaphore()

    def hello(device):
        pl.semaphore_signal(barrier, inc=1, device_id=device, device_id_type=MESH)

    for peer in (left, right, other(t)):
        hello({"tp": peer})

    @pl.loop(0, n_sp)
    def _(r):
        @pl.when(r != s)
        def _():
            hello({"sp": r, "tp": t})

        @pl.when(jnp.logical_or(r != s, t != source))
        def _():
            hello({"sp": r, "tp": source})

    own = jnp.logical_or(row_of(2 * t) == s, row_of(2 * t + 1) == s)
    pl.semaphore_wait(barrier, 3 + n_sp - 1 + 2 * n_tp - own.astype(jnp.int32))

    def pieces(u, hi):
        there = lax.rem(t + u, n_tp)
        rows, cols = pl.ds(there * sub, sub), pl.ds(hi * HEAD, HEAD)
        return there, (
            (q_ref.at[rows, cols], qbuf.at[s], 0, recv_a.at[n_sp]),
            (f_ref.at[hi], fbuf.at[s], 1, recv_a.at[n_sp + 1]),
            (k_ref.at[rows, cols], kv.at[s, there, 0], 2, recv_a.at[s]),
            (v_ref.at[rows, cols], kv.at[s, there, 1], 3, recv_a.at[s]),
        )

    def each_piece(act, start):
        @pl.loop(0, n_tp)
        def _(u):
            for hi in range(2):
                r = row_of(2 * t + hi)
                there, list_of = pieces(u, hi)
                mine = jnp.logical_and(r == s, there == t)

                @pl.when(jnp.logical_not(mine))
                def _():
                    for src, dst, i, sem in list_of:
                        act(remote(src, dst, send_a.at[hi, u, i], sem, {"sp": r, "tp": there}))

                if start:

                    @pl.when(mine)
                    def _():
                        for src, dst, _, sem in list_of:
                            pltpu.make_async_copy(src, dst, sem).start()

    each_piece(lambda c: c.start(), True)

    to_left, to_right, to_other = {"tp": left}, {"tp": right}, {"tp": other(t)}

    def at_step(j):
        d = (j + 1) // 2
        return lax.rem(s + n_sp + jnp.where(lax.rem(j, 2) == 1, d, -d), n_sp)

    def stage_one(j):
        b = at_step(j)
        arrived(kv.at[b, t], recv_a.at[b], to_other)
        piece = kv.at[b, t]
        remote(piece, piece, send_b.at[0], recv_b.at[0, b], to_right).start()
        remote(piece, piece, send_b.at[1], recv_b.at[1, b], to_left).start()
        remote(piece, piece, send_b.at[2], recv_c.at[0], to_other).start()

    def stage_two(j):
        b = at_step(j)
        arrived(kv.at[b, left], recv_b.at[0, b], to_left)
        piece, part = kv.at[b, left], kv.at[b, left, 0]
        remote(part, part, send_b.at[3], recv_b.at[2, b], to_right).start()
        remote(piece, piece, send_c.at[0], recv_c.at[1], to_other).start()
        arrived(kv.at[b, right], recv_b.at[1, b], to_right)
        piece, part = kv.at[b, right], kv.at[b, right, 1]
        remote(part, part, send_b.at[4], recv_b.at[3, b], to_left).start()
        remote(piece, piece, send_c.at[1], recv_c.at[2], to_other).start()

    def stage_three(j):
        b = at_step(j)
        arrived(kv.at[b, opp, 0], recv_b.at[2, b], to_left)
        part = kv.at[b, opp, 0]
        remote(part, part, send_c.at[2], recv_c.at[3], to_other).start()
        arrived(kv.at[b, opp, 1], recv_b.at[3, b], to_right)
        part = kv.at[b, opp, 1]
        remote(part, part, send_c.at[3], recv_c.at[4], to_other).start()

    lag = 2

    @pl.loop(0, n_sp + 2 * lag)
    def _(j):
        @pl.when(j < n_sp)
        def _():
            stage_one(j)

        @pl.when(jnp.logical_and(j >= lag, j < n_sp + lag))
        def _():
            stage_two(j - lag)

        @pl.when(j >= 2 * lag)
        def _():
            stage_three(j - 2 * lag)

    arrived(kv.at[:, other(t)], recv_c.at[0], to_other)
    arrived(kv.at[:, other(left)], recv_c.at[1], to_other)
    arrived(kv.at[:, other(right)], recv_c.at[2], to_other)
    arrived(kv.at[:, other(opp), 0], recv_c.at[3], to_other)
    arrived(kv.at[:, other(opp), 1], recv_c.at[4], to_other)
    arrived(qbuf, recv_a.at[n_sp], to_other)
    arrived(fbuf, recv_a.at[n_sp + 1], to_other)

    width = n_tp * sub

    @pl.loop(0, n_sp)
    def _(b):
        rows = kv[b, :, 0].reshape(width, HEAD).astype(jnp.float32)
        kn[b] = normed(rows, kg_ref[...]).astype(jnp.bfloat16)

    group = 4
    tall, wide = group * sub, group * width
    factor = LOG2E / math.sqrt(HEAD)

    def bias_row(c, base):
        parts = []
        for b in range(group):
            slab = fbuf[c * group + b]
            for lane in range(width // HEAD):
                parts.append(slab[lane : lane + 1])
        return (base - jnp.concatenate(parts, axis=1)) * LOG2E

    @pl.loop(0, n_sp // group)
    def _(step):
        i = n_sp // group - 1 - step
        q = qbuf[pl.ds(i * group, group)].reshape(tall, HEAD).astype(jnp.float32)
        q = normed(q, qg_ref[...]).astype(jnp.bfloat16)
        base = fbuf[i * group, 0:1, 0:1]

        def visit(c, state, masked):
            top, total, acc = state
            keys = kn[pl.ds(c * group, group)].reshape(wide, HEAD)
            scores = lax.dot_general(q, keys, (((1,), (1,)), ((), ())), preferred_element_type=jnp.float32)
            scores = scores * factor + bias_row(c, base)
            if masked:
                line = lax.broadcasted_iota(jnp.int32, (tall, wide), 0)
                place = (line // sub) * width + t * sub + lax.rem(line, sub)
                scores = jnp.where(lax.broadcasted_iota(jnp.int32, (tall, wide), 1) <= place, scores, LOW)
            high = jnp.maximum(top, jnp.max(scores, axis=1, keepdims=True))
            raised = jnp.exp2(scores - high)
            shrink = jnp.exp2(top - high)
            total = total * shrink + jnp.sum(raised, axis=1, keepdims=True)
            vals = kv[pl.ds(c * group, group), :, 1].reshape(wide, HEAD)
            acc = acc * shrink + jnp.dot(raised.astype(jnp.bfloat16), vals, preferred_element_type=jnp.float32)
            return high, total, acc

        state = (
            jnp.full((tall, 1), LOW, jnp.float32),
            jnp.zeros((tall, 1), jnp.float32),
            jnp.zeros((tall, HEAD), jnp.float32),
        )
        state = visit(i, state, True)
        _, total, acc = lax.fori_loop(0, i, lambda c, st: visit(c, st, False), state)
        obuf[pl.ds(i * group, group)] = (acc / total).astype(jnp.bfloat16).reshape(group, sub, HEAD)

        @pl.loop(0, group)
        def _(n):
            r = i * group + n
            cols = pl.ds(pl.multiple_of(my_head * HEAD, HEAD), HEAD)

            @pl.when(r != s)
            def _():
                remote(obuf.at[r], att.at[t, :, cols], send_o.at[r], recv_o, {"sp": r, "tp": t}).start()

            @pl.when(r == s)
            def _():
                att[t, :, cols] = obuf[r]

    def o_wait(r):
        @pl.when(r != s)
        def _():
            left_over(obuf.at[r], send_o.at[r], {"sp": r, "tp": t})

    pl.loop(0, n_sp)(o_wait)
    arrived(att.at[t, :, pl.ds(0, (n_sp - 1) * HEAD)], recv_o, to_other)

    row_gather(row, att, send_g.at[0], recv_g.at[0])
    total_rows = n_tp * sub
    span = 256

    @pl.loop(0, total_rows // span)
    def _(m):
        rows = pl.ds(m * span, span)
        lhs = att[pl.ds(m * (span // sub), span // sub)].reshape(span, att.shape[2])
        product = jnp.dot(lhs, ow_ref[...], preferred_element_type=jnp.float32)
        mid[t, rows] = (res_ref[rows].astype(jnp.float32) + product).astype(jnp.bfloat16)

    row_gather(row, mid, send_g.at[1], recv_g.at[1])
    out = pltpu.make_async_copy(mid, out_ref, out_sem)
    out.start()

    each_piece(lambda c: c.wait_send(), False)
    left_over(kv.at[:, t], send_b.at[0], to_right)
    left_over(kv.at[:, t], send_b.at[1], to_left)
    left_over(kv.at[:, t], send_b.at[2], to_other)
    left_over(kv.at[:, left, 0], send_b.at[3], to_right)
    left_over(kv.at[:, right, 1], send_b.at[4], to_left)
    left_over(kv.at[:, left], send_c.at[0], to_other)
    left_over(kv.at[:, right], send_c.at[1], to_other)
    left_over(kv.at[:, opp, 0], send_c.at[2], to_other)
    left_over(kv.at[:, opp, 1], send_c.at[3], to_other)
    out.wait()


def feed_forward_kernel(
    n_sp,
    n_tp,
    mid_ref,
    w_ref,
    gain_ref,
    out_ref,
    mid,
    wg,
    wu,
    wd,
    nrm,
    hid,
    part,
    pair,
    total,
    landed,
    load_sem,
    send_p,
    recv_p,
    send_r,
    recv_r,
):
    t = lax.axis_index("tp")
    row = Row(t, n_tp)
    other = Row.other
    left, right, opp, core = row.left, row.right, row.opp, row.core
    ff = wg.shape[0]
    cols = mid.shape[2]
    depth = w_ref.shape[2]
    rows = mid.shape[1]

    loads = [pltpu.make_async_copy(mid_ref, mid, load_sem.at[0])]
    for i, w in enumerate((wg, wu, wd)):
        for z in range(n_sp):
            loads.append(
                pltpu.make_async_copy(
                    w_ref.at[z, pl.ds(i * ff, ff)], w.at[:, pl.ds(z * depth, depth)], load_sem.at[1 + i * n_sp + z]
                )
            )
    for load in loads:
        load.start()

    barrier = pltpu.get_barrier_semaphore()
    for peer in (left, right, opp, other(t)):
        pl.semaphore_signal(barrier, inc=1, device_id={"tp": peer}, device_id_type=MESH)
    pl.semaphore_wait(barrier, 4)

    loads[0].wait()
    span = 128

    @pl.loop(0, rows // span)
    def _(m):
        at = pl.ds(m * span, span)
        blocks = [mid[u, at].astype(jnp.float32) for u in range(n_tp)]
        square = sum(jnp.sum(b * b, axis=1, keepdims=True) for b in blocks) / (n_tp * cols)
        scale = lax.rsqrt(square + EPS)
        for u in range(n_tp):
            nrm[at, pl.ds(u * cols, cols)] = (blocks[u] * scale * gain_ref[u]).astype(jnp.bfloat16)

    for load in loads[1:]:
        load.wait()
    tall = 256

    @pl.loop(0, rows // tall)
    def _(m):
        at = pl.ds(m * tall, tall)
        across = (((1,), (1,)), ((), ()))
        gate = lax.dot_general(nrm[at], wg[...], across, preferred_element_type=jnp.float32)
        up = lax.dot_general(nrm[at], wu[...], across, preferred_element_type=jnp.float32)
        hid[at] = (gate / (1.0 + jnp.exp(-gate)) * up).astype(jnp.bfloat16)

    to_other = {"tp": other(t)}
    chips = (opp, right, left, t)

    def add(k):
        arrived(pair.at[k], recv_p.at[k], to_other)
        mine = part[k, core].astype(jnp.float32) + pair[k].astype(jnp.float32)
        if k < 3:
            total[k] = mine.astype(jnp.bfloat16)
            remote(total.at[k], landed.at[k], send_r.at[k], recv_r.at[k], {"tp": chips[k]}).start()
            return None
        return mine

    for k in range(4):
        base = (chips[k] - core) * cols
        for side in range(2):
            at = pl.ds(pl.multiple_of(base + side * cols, cols), cols)
            part[k, side] = jnp.dot(hid[...], wd[:, at], preferred_element_type=jnp.float32).astype(jnp.bfloat16)
        remote(part.at[k, 1 - core], pair.at[k], send_p.at[k], recv_p.at[k], to_other).start()
        if k > 0:
            add(k - 1)
    mine = add(3) + mid[t].astype(jnp.float32)
    for k in (1, 2, 0):
        arrived(landed.at[k], recv_r.at[k], to_other)
        mine = mine + landed[k].astype(jnp.float32)
    out_ref[...] = mine.astype(jnp.bfloat16)
    for k in range(4):
        left_over(part.at[k, 1 - core], send_p.at[k], to_other)
    for k in range(3):
        left_over(total.at[k], send_r.at[k], {"tp": chips[k]})


def local(n_sp, n_tp, q, k, v, f, res, qg, kg, ow, ng, gw, uw, dw):
    rows, cols = q.shape
    sub = rows // n_tp
    hbm = pl.BlockSpec(memory_space=pltpu.HBM)
    vmem = pl.BlockSpec(memory_space=pltpu.VMEM)
    dma = pltpu.SemaphoreType.DMA
    flat = jnp.concatenate((gw, uw, dw), axis=1).T
    w = lax.all_gather(flat, "sp", axis=0)
    f = jnp.pad(f.T.reshape(2, rows // HEAD, HEAD), ((0, 0), (0, 8 - rows // HEAD), (0, 0)))
    bf = jnp.bfloat16
    width = n_sp * HEAD
    mid = pl.pallas_call(
        functools.partial(attention_kernel, n_sp, n_tp),
        out_shape=jax.ShapeDtypeStruct((n_tp, rows, cols), bf),
        in_specs=[hbm] * 4 + [vmem] * 4,
        out_specs=hbm,
        scratch_shapes=[
            pltpu.VMEM((n_sp, sub, HEAD), bf),
            pltpu.VMEM((n_sp, n_tp, 2, sub, HEAD), bf),
            pltpu.VMEM((n_sp, 8, HEAD), jnp.float32),
            pltpu.VMEM((n_sp, rows, HEAD), bf),
            pltpu.VMEM((n_sp, sub, HEAD), bf),
            pltpu.VMEM((n_tp, sub, width), bf),
            pltpu.VMEM((n_tp, rows, cols), bf),
            dma((2, n_tp, 4)),
            dma((n_sp + 2,)),
            dma((5,)),
            dma((4, n_sp)),
            dma((4,)),
            dma((5,)),
            dma((n_sp,)),
            dma,
            dma((2, 9)),
            dma((2, 9)),
            dma,
        ],
        compiler_params=pltpu.CompilerParams(
            collective_id=0, has_side_effects=True, vmem_limit_bytes=48 * 1024 * 1024
        ),
        cost_estimate=pl.CostEstimate(flops=40_000_000_000, bytes_accessed=100_000_000, transcendentals=0),
        name="attend",
    )(q, k, v, f, res, ow, qg.reshape(1, HEAD), kg.reshape(1, HEAD))
    ff = gw.shape[1]
    deep = n_tp * cols
    return pl.pallas_call(
        functools.partial(feed_forward_kernel, n_sp, n_tp),
        out_shape=jax.ShapeDtypeStruct((rows, cols), bf),
        in_specs=[hbm, hbm, vmem],
        out_specs=vmem,
        scratch_shapes=[
            pltpu.VMEM((n_tp, rows, cols), bf),
            pltpu.VMEM((ff, deep), bf),
            pltpu.VMEM((ff, deep), bf),
            pltpu.VMEM((ff, deep), bf),
            pltpu.VMEM((rows, deep), bf),
            pltpu.VMEM((rows, ff), bf),
            pltpu.VMEM((4, 2, rows, cols), bf),
            pltpu.VMEM((4, rows, cols), bf),
            pltpu.VMEM((3, rows, cols), bf),
            pltpu.VMEM((3, rows, cols), bf),
            dma((1 + 3 * n_sp,)),
            dma((4,)),
            dma((4,)),
            dma((3,)),
            dma((3,)),
        ],
        compiler_params=pltpu.CompilerParams(
            collective_id=1, has_side_effects=True, vmem_limit_bytes=48 * 1024 * 1024
        ),
        cost_estimate=pl.CostEstimate(flops=4_400_000_000, bytes_accessed=12_000_000, transcendentals=0),
        name="feed",
    )(mid, w, ng.reshape(n_tp, 1, cols))


def solution(mesh):
    whole = P(("grp", "sp"), "tp")
    weight = P("sp", "tp")
    placed = (whole,) * 5 + (P(), P(), P(None, "tp"), P(), weight, weight, weight)
    return jax.shard_map(
        functools.partial(local, mesh.shape["sp"], mesh.shape["tp"]),
        mesh=mesh,
        in_specs=placed,
        out_specs=whole,
        check_vma=False,
    )
```

time: 328 us -> 228 us (0.70)
  the two profiles are of different devices: /device:TPU:1568 before, /device:TPU:33 now
where the time goes in v1:
time: 228 us
  Pallas kernels  207 us (91%)
  between operations  13.5 us (6%)
  local copies, waits for them, and re-layouts  5.61 us (2%)
    pallas_call x1, Pallas kernels, local(): pl.pallas_call(functools.partial(attention_kernel, n_sp, n_tp), out_shape...  182 us
    pallas_call x1, Pallas kernels, local(): pl.pallas_call(functools.partial(feed_forward_kernel, n_sp, n_tp), out_sh...  25.1 us
    unnamed x23, local copies, waits for them, and re-layouts  5.59 us
  transfers between devices with their start and end apart: 1, of which 0 were waited for; matrix products, arithmetic and copies ran while one was open for 0% of the time, Pallas kernels for 80%

profile of v1, /device:TPU:33, one launch (start us, length us, event | category | flops | bytes accessed | tf_op | source)
XLA Modules:
  0.0 228.2 jit_solution(438955765281415716)
XLA Ops:
  6.5 0.0 copy-start.10
  6.5 0.0 copy-start
  6.6 0.0 copy-start.7
  6.6 0.0 copy-start.6
  6.6 0.0 copy-start.2
  6.6 0.0 copy-start.1
  6.6 0.1 all-gather.3.cloned.1.call-start
  6.6 2.0 maximum_bitcast_fusion
  8.7 0.1 all-gather.3.cloned.1.call-update
  8.7 0.0 copy-done.10
  8.8 0.0 copy-done
  8.8 0.0 copy-done.7
  8.8 0.0 copy-done.6
  8.8 0.0 copy-done.2
  8.8 0.0 copy-done.1
  8.8 0.0 copy-start.3
  8.8 0.9 copy-done.3
  9.8 0.0 copy-start.4
  9.8 0.9 copy-done.4
  10.7 0.0 copy-start.5
  10.7 181.8 %attend.1.mid_ref = bf16[8,512,256]{2,1,0:T(8,128)(2,1)S(1)} custom-call(bf16[512,256]{1,0:T(8,128)(2,1)S(1)} %copy-done.1, bf16[512,256]{1,0:T(8,128)(2,1)S(1)} %copy-done.2, bf16[512,256]{1,0:T(8,128)(2,1)S(1)} %copy-done.3, f32[2,8,128]{2,1,0:T(8,128)S(1)} %pad.4.f_ref, bf16[512,256]{1,0:T(8,128)(2,1)S(1)} %copy-done.4, bf16[2048,256]{1,0:T(8,128)(2,1)S(1)} %copy-done, ...), custom_call_target="tpu_custom_call" | custom-call | flops 40000000000 | bytes 100000000 | tf_op jit(solution)/shard_map/attend/pallas_call | solution.py:459
  192.5 0.0 copy-start.8
  192.5 1.4 copy-done.8
  193.9 0.0 all-gather.3.cloned.1.call-done
  193.9 0.0 copy-done.5
  193.9 0.0 copy-start.9
  193.9 1.6 copy-done.9
  195.5 25.1 %feed.1 = bf16[512,256]{1,0:T(8,128)(2,1)S(1)} custom-call(bf16[8,512,256]{2,1,0:T(8,128)(2,1)S(1)} %copy-done.9, bf16[16,2064,128]{2,1,0:T(8,128)(2,1)} %bitcast.11, f32[8,1,256]{2,1,0:T(1,128)S(1)} %bitcast.7), custom_call_target="tpu_custom_call" | custom-call | flops 4400000000 | bytes 12000000 | tf_op jit(solution)/shard_map/feed/pallas_call | solution.py:492
  220.6 0.7 copy.14
  (2 shorter events, 0.0 us)
Async XLA Ops:
  6.5 2.2 copy-start.10
  6.5 2.2 copy-start
  6.6 2.2 copy-start.7
  6.6 2.2 copy-start.6
  6.6 2.2 copy-start.2
  6.6 2.3 copy-start.1
  6.6 187.3 %all-gather.3.cloned.1.call-start = ((), (), s32[]{:S(2)}) async-start(), calls=%async_computation | async-start | bytes 8982528 | tf_op jit(solution)/shard_map/all_gather | solution.py:455
  8.8 1.0 copy-start.3
  9.8 0.9 copy-start.4
  10.7 183.2 %copy-start.5 = (f32[2048]{0:T(1024)S(1)}, f32[2048]{0:T(1024)}, u32[]{:S(2)}) copy-start(f32[2048]{0:T(1024)} %param.20) | copy-start | bytes 24580
  192.5 1.4 copy-start.8
  193.9 1.6 copy-start.9
Sparse Core Ops, SparseCore 0:
  9.2 180.5 all-gather.2

commit v2 on v1

--- a/solution.py
+++ b/solution.py
@@ -82,7 +82,7 @@
     return rows * lax.rsqrt(square + EPS) * gain
 
 
-def attention_kernel(
+def layer_kernel(
     n_sp,
     n_tp,
     q_ref,
@@ -93,6 +93,8 @@
     ow_ref,
     qg_ref,
     kg_ref,
+    w_ref,
+    gain_ref,
     out_ref,
     qbuf,
     kv,
@@ -111,9 +113,28 @@
     recv_o,
     send_g,
     recv_g,
-    out_sem,
+    wbuf,
+    nrm,
+    hid,
+    part,
+    pair,
+    total,
+    landed,
+    own_sem,
+    send_w,
+    recv_w,
+    send_y,
+    recv_y,
+    send_p,
+    recv_p,
+    send_r,
+    recv_r,
 ):
     s = lax.axis_index("sp")
+    parity = lax.rem(lax.axis_index("grp"), 2)
+    to_pair = {"grp": lax.axis_index("grp") + 1 - 2 * parity}
+    to_next = {"sp": lax.rem(s + 1, n_sp)}
+    to_last = {"sp": lax.rem(s + n_sp - 1, n_sp)}
     t = lax.axis_index("tp")
     row = Row(t, n_tp)
     other = Row.other
@@ -135,8 +156,9 @@
     def hello(device):
         pl.semaphore_signal(barrier, inc=1, device_id=device, device_id_type=MESH)
 
-    for peer in (left, right, other(t)):
+    for peer in (left, right, opp, other(t)):
         hello({"tp": peer})
+    hello(to_pair)
 
     @pl.loop(0, n_sp)
     def _(r):
@@ -149,24 +171,27 @@
             hello({"sp": r, "tp": source})
 
     own = jnp.logical_or(row_of(2 * t) == s, row_of(2 * t + 1) == s)
-    pl.semaphore_wait(barrier, 3 + n_sp - 1 + 2 * n_tp - own.astype(jnp.int32))
-
-    def pieces(u, hi):
+    pl.semaphore_wait(barrier, 5 + n_sp - 1 + 2 * n_tp - own.astype(jnp.int32))
+
+    def pieces(u, hi, keys):
         there = lax.rem(t + u, n_tp)
         rows, cols = pl.ds(there * sub, sub), pl.ds(hi * HEAD, HEAD)
+        if keys:
+            return there, (
+                (k_ref.at[rows, cols], kv.at[s, there, 0], 2, recv_a.at[s]),
+                (v_ref.at[rows, cols], kv.at[s, there, 1], 3, recv_a.at[s]),
+            )
         return there, (
             (q_ref.at[rows, cols], qbuf.at[s], 0, recv_a.at[n_sp]),
             (f_ref.at[hi], fbuf.at[s], 1, recv_a.at[n_sp + 1]),
-            (k_ref.at[rows, cols], kv.at[s, there, 0], 2, recv_a.at[s]),
-            (v_ref.at[rows, cols], kv.at[s, there, 1], 3, recv_a.at[s]),
         )
 
-    def each_piece(act, start):
+    def each_piece(act, start, keys):
         @pl.loop(0, n_tp)
         def _(u):
             for hi in range(2):
                 r = row_of(2 * t + hi)
-                there, list_of = pieces(u, hi)
+                there, list_of = pieces(u, hi, keys)
                 mine = jnp.logical_and(r == s, there == t)
 
                 @pl.when(jnp.logical_not(mine))
@@ -181,7 +206,46 @@
                         for src, dst, _, sem in list_of:
                             pltpu.make_async_copy(src, dst, sem).start()
 
-    each_piece(lambda c: c.start(), True)
+    third = w_ref.shape[0] // 3
+    ringed = pl.ds(pl.multiple_of(parity * third, 16), 2 * third)
+    shared = pl.ds(pl.multiple_of(parity * 2 * third, 16), third)
+    half_way = n_sp // 2
+
+    def chunk(d):
+        return lax.rem(s + d + n_sp, n_sp)
+
+    def pass_on(k, src, chunk_at, to, way):
+        remote(src, wbuf.at[chunk_at, ringed], send_w.at[way, k], recv_w.at[way, k], to).start()
+
+    def tick(k):
+        here = chunk(-k)
+        arrived(wbuf.at[here, ringed], recv_w.at[0, k - 1], to_last)
+
+        @pl.when(k < half_way)
+        def _():
+            pass_on(k, wbuf.at[here, ringed], here, to_next, 0)
+
+        piece = wbuf.at[here, shared]
+        remote(piece, piece, send_y, recv_y, to_pair).start()
+
+        @pl.when(k < half_way)
+        def _():
+            far = chunk(k)
+            arrived(wbuf.at[far, ringed], recv_w.at[1, k - 1], to_next)
+
+            @pl.when(k < half_way - 1)
+            def _():
+                pass_on(k, wbuf.at[far, ringed], far, to_last, 1)
+
+            piece = wbuf.at[far, shared]
+            remote(piece, piece, send_y, recv_y, to_pair).start()
+
+    own_copy = pltpu.make_async_copy(w_ref, wbuf.at[s], own_sem)
+    own_copy.start()
+    each_piece(lambda c: c.start(), True, True)
+    pass_on(0, w_ref.at[ringed], s, to_next, 0)
+    pass_on(0, w_ref.at[ringed], s, to_last, 1)
+    each_piece(lambda c: c.start(), True, False)
 
     to_left, to_right, to_other = {"tp": left}, {"tp": right}, {"tp": other(t)}
 
@@ -232,6 +296,10 @@
         @pl.when(j >= 2 * lag)
         def _():
             stage_three(j - 2 * lag)
+
+        @pl.when(lax.rem(j, 4) == 3)
+        def _():
+            tick(j // 4 + 1)
 
     arrived(kv.at[:, other(t)], recv_c.at[0], to_other)
     arrived(kv.at[:, other(left)], recv_c.at[1], to_other)
@@ -306,6 +374,8 @@
             def _():
                 att[t, :, cols] = obuf[r]
 
+    tick(6)
+
     def o_wait(r):
         @pl.when(r != s)
         def _():
@@ -314,7 +384,9 @@
     pl.loop(0, n_sp)(o_wait)
     arrived(att.at[t, :, pl.ds(0, (n_sp - 1) * HEAD)], recv_o, to_other)
 
+    tick(7)
     row_gather(row, att, send_g.at[0], recv_g.at[0])
+    tick(8)
     total_rows = n_tp * sub
     span = 256
 
@@ -326,71 +398,10 @@
         mid[t, rows] = (res_ref[rows].astype(jnp.float32) + product).astype(jnp.bfloat16)
 
     row_gather(row, mid, send_g.at[1], recv_g.at[1])
-    out = pltpu.make_async_copy(mid, out_ref, out_sem)
-    out.start()
-
-    each_piece(lambda c: c.wait_send(), False)
-    left_over(kv.at[:, t], send_b.at[0], to_right)
-    left_over(kv.at[:, t], send_b.at[1], to_left)
-    left_over(kv.at[:, t], send_b.at[2], to_other)
-    left_over(kv.at[:, left, 0], send_b.at[3], to_right)
-    left_over(kv.at[:, right, 1], send_b.at[4], to_left)
-    left_over(kv.at[:, left], send_c.at[0], to_other)
-    left_over(kv.at[:, right], send_c.at[1], to_other)
-    left_over(kv.at[:, opp, 0], send_c.at[2], to_other)
-    left_over(kv.at[:, opp, 1], send_c.at[3], to_other)
-    out.wait()
-
-
-def feed_forward_kernel(
-    n_sp,
-    n_tp,
-    mid_ref,
-    w_ref,
-    gain_ref,
-    out_ref,
-    mid,
-    wg,
-    wu,
-    wd,
-    nrm,
-    hid,
-    part,
-    pair,
-    total,
-    landed,
-    load_sem,
-    send_p,
-    recv_p,
-    send_r,
-    recv_r,
-):
-    t = lax.axis_index("tp")
-    row = Row(t, n_tp)
-    other = Row.other
-    left, right, opp, core = row.left, row.right, row.opp, row.core
-    ff = wg.shape[0]
     cols = mid.shape[2]
-    depth = w_ref.shape[2]
     rows = mid.shape[1]
-
-    loads = [pltpu.make_async_copy(mid_ref, mid, load_sem.at[0])]
-    for i, w in enumerate((wg, wu, wd)):
-        for z in range(n_sp):
-            loads.append(
-                pltpu.make_async_copy(
-                    w_ref.at[z, pl.ds(i * ff, ff)], w.at[:, pl.ds(z * depth, depth)], load_sem.at[1 + i * n_sp + z]
-                )
-            )
-    for load in loads:
-        load.start()
-
-    barrier = pltpu.get_barrier_semaphore()
-    for peer in (left, right, opp, other(t)):
-        pl.semaphore_signal(barrier, inc=1, device_id={"tp": peer}, device_id_type=MESH)
-    pl.semaphore_wait(barrier, 4)
-
-    loads[0].wait()
+    core = row.core
+    depth = wbuf.shape[2]
     span = 128
 
     @pl.loop(0, rows // span)
@@ -402,19 +413,22 @@
         for u in range(n_tp):
             nrm[at, pl.ds(u * cols, cols)] = (blocks[u] * scale * gain_ref[u]).astype(jnp.bfloat16)
 
-    for load in loads[1:]:
-        load.wait()
+    own_copy.wait()
+    arrived(wbuf.at[pl.ds(0, n_sp - 1), shared], recv_y, to_pair)
+
+    def stacked(which, first, count):
+        return jnp.concatenate([wbuf[first + z, pl.ds(which * third, third)] for z in range(count)], axis=1)
+
     tall = 256
 
     @pl.loop(0, rows // tall)
     def _(m):
         at = pl.ds(m * tall, tall)
         across = (((1,), (1,)), ((), ()))
-        gate = lax.dot_general(nrm[at], wg[...], across, preferred_element_type=jnp.float32)
-        up = lax.dot_general(nrm[at], wu[...], across, preferred_element_type=jnp.float32)
+        gate = lax.dot_general(nrm[at], stacked(0, 0, n_sp), across, preferred_element_type=jnp.float32)
+        up = lax.dot_general(nrm[at], stacked(1, 0, n_sp), across, preferred_element_type=jnp.float32)
         hid[at] = (gate / (1.0 + jnp.exp(-gate)) * up).astype(jnp.bfloat16)
 
-    to_other = {"tp": other(t)}
     chips = (opp, right, left, t)
 
     def add(k):
@@ -427,10 +441,10 @@
         return mine
 
     for k in range(4):
-        base = (chips[k] - core) * cols
+        each = cols // depth
         for side in range(2):
-            at = pl.ds(pl.multiple_of(base + side * cols, cols), cols)
-            part[k, side] = jnp.dot(hid[...], wd[:, at], preferred_element_type=jnp.float32).astype(jnp.bfloat16)
+            down = stacked(2, (chips[k] - core + side) * each, each)
+            part[k, side] = jnp.dot(hid[...], down, preferred_element_type=jnp.float32).astype(jnp.bfloat16)
         remote(part.at[k, 1 - core], pair.at[k], send_p.at[k], recv_p.at[k], to_other).start()
         if k > 0:
             add(k - 1)
@@ -443,6 +457,22 @@
         left_over(part.at[k, 1 - core], send_p.at[k], to_other)
     for k in range(3):
         left_over(total.at[k], send_r.at[k], {"tp": chips[k]})
+    each_piece(lambda c: c.wait_send(), False, True)
+    each_piece(lambda c: c.wait_send(), False, False)
+    left_over(kv.at[:, t], send_b.at[0], to_right)
+    left_over(kv.at[:, t], send_b.at[1], to_left)
+    left_over(kv.at[:, t], send_b.at[2], to_other)
+    left_over(kv.at[:, left, 0], send_b.at[3], to_right)
+    left_over(kv.at[:, right, 1], send_b.at[4], to_left)
+    left_over(kv.at[:, left], send_c.at[0], to_other)
+    left_over(kv.at[:, right], send_c.at[1], to_other)
+    left_over(kv.at[:, opp, 0], send_c.at[2], to_other)
+    left_over(kv.at[:, opp, 1], send_c.at[3], to_other)
+    for k in range(half_way):
+        left_over(wbuf.at[s, ringed], send_w.at[0, k], to_next)
+    for k in range(half_way - 1):
+        left_over(wbuf.at[s, ringed], send_w.at[1, k], to_last)
+    left_over(wbuf.at[pl.ds(0, n_sp - 1), shared], send_y, to_pair)
 
 
 def local(n_sp, n_tp, q, k, v, f, res, qg, kg, ow, ng, gw, uw, dw):
@@ -452,15 +482,15 @@
     vmem = pl.BlockSpec(memory_space=pltpu.VMEM)
     dma = pltpu.SemaphoreType.DMA
     flat = jnp.concatenate((gw, uw, dw), axis=1).T
-    w = lax.all_gather(flat, "sp", axis=0)
     f = jnp.pad(f.T.reshape(2, rows // HEAD, HEAD), ((0, 0), (0, 8 - rows // HEAD), (0, 0)))
     bf = jnp.bfloat16
     width = n_sp * HEAD
-    mid = pl.pallas_call(
-        functools.partial(attention_kernel, n_sp, n_tp),
-        out_shape=jax.ShapeDtypeStruct((n_tp, rows, cols), bf),
-        in_specs=[hbm] * 4 + [vmem] * 4,
-        out_specs=hbm,
+    ff = gw.shape[1]
+    return pl.pallas_call(
+        functools.partial(layer_kernel, n_sp, n_tp),
+        out_shape=jax.ShapeDtypeStruct((rows, cols), bf),
+        in_specs=[hbm] * 4 + [vmem] * 4 + [hbm, vmem],
+        out_specs=vmem,
         scratch_shapes=[
             pltpu.VMEM((n_sp, sub, HEAD), bf),
             pltpu.VMEM((n_sp, n_tp, 2, sub, HEAD), bf),
@@ -479,44 +509,29 @@
             dma,
             dma((2, 9)),
             dma((2, 9)),
-            dma,
-        ],
-        compiler_params=pltpu.CompilerParams(
-            collective_id=0, has_side_effects=True, vmem_limit_bytes=48 * 1024 * 1024
-        ),
-        cost_estimate=pl.CostEstimate(flops=40_000_000_000, bytes_accessed=100_000_000, transcendentals=0),
-        name="attend",
-    )(q, k, v, f, res, ow, qg.reshape(1, HEAD), kg.reshape(1, HEAD))
-    ff = gw.shape[1]
-    deep = n_tp * cols
-    return pl.pallas_call(
-        functools.partial(feed_forward_kernel, n_sp, n_tp),
-        out_shape=jax.ShapeDtypeStruct((rows, cols), bf),
-        in_specs=[hbm, hbm, vmem],
-        out_specs=vmem,
-        scratch_shapes=[
-            pltpu.VMEM((n_tp, rows, cols), bf),
-            pltpu.VMEM((ff, deep), bf),
-            pltpu.VMEM((ff, deep), bf),
-            pltpu.VMEM((ff, deep), bf),
-            pltpu.VMEM((rows, deep), bf),
+            pltpu.VMEM((n_sp, 3 * ff, gw.shape[0]), bf),
+            pltpu.VMEM((rows, n_tp * cols), bf),
             pltpu.VMEM((rows, ff), bf),
             pltpu.VMEM((4, 2, rows, cols), bf),
             pltpu.VMEM((4, rows, cols), bf),
             pltpu.VMEM((3, rows, cols), bf),
             pltpu.VMEM((3, rows, cols), bf),
-            dma((1 + 3 * n_sp,)),
+            dma,
+            dma((2, n_sp // 2)),
+            dma((2, n_sp // 2)),
+            dma,
+            dma,
             dma((4,)),
             dma((4,)),
             dma((3,)),
             dma((3,)),
         ],
         compiler_params=pltpu.CompilerParams(
-            collective_id=1, has_side_effects=True, vmem_limit_bytes=48 * 1024 * 1024
+            collective_id=0, has_side_effects=True, vmem_limit_bytes=60 * 1024 * 1024
         ),
-        cost_estimate=pl.CostEstimate(flops=4_400_000_000, bytes_accessed=12_000_000, transcendentals=0),
-        name="feed",
-    )(mid, w, ng.reshape(n_tp, 1, cols))
+        cost_estimate=pl.CostEstimate(flops=40_000_000_000, bytes_accessed=100_000_000, transcendentals=0),
+        name="layer",
+    )(q, k, v, f, res, ow, qg.reshape(1, HEAD), kg.reshape(1, HEAD), flat, ng.reshape(n_tp, 1, cols))
 
 
 def solution(mesh):

time: 228 us -> 217 us (0.952)
  between operations: 13.5 us -> 0.01 us
  Pallas kernels: 207 us -> 211 us
  local copies, waits for them, and re-layouts: 5.61 us -> 2.97 us
    pallas_call x2 -> x1, Pallas kernels: 207 us -> 211 us  [local(): pl.pallas_call(functools.partial(layer_kernel, n_sp, n_tp), out_shape=jax...]
    unnamed x23 -> x1, local copies, waits for them, and re-layouts: 5.59 us -> 1.67 us
  transfers between devices with their start and end apart: 1 -> 0, of which waited for: 0 -> 0; matrix products, arithmetic and copies ran while one was open for 0% -> 0% of each run, Pallas kernels for 80% -> 0%
where the time goes in v2:
time: 217 us; the launch traced here: 216 us
  Pallas kernels  211 us (97%)
  local copies, waits for them, and re-layouts  2.97 us (1%)
    pallas_call x1, Pallas kernels, local(): pl.pallas_call(functools.partial(layer_kernel, n_sp, n_tp), out_shape=jax...  211 us

profile of v2, /device:TPU:33, one launch (start us, length us, event | category | flops | bytes accessed | tf_op | source)
XLA Modules:
  0.0 216.3 jit_solution(6464386616696473094)
XLA Ops:
  0.0 0.7 reshape.12
  0.7 0.6 pad.4.f_ref
  1.3 1.9 maximum_bitcast_fusion.w_ref
  3.2 211.4 %layer.1 = bf16[512,256]{1,0:T(8,128)(2,1)} custom-call(bf16[512,256]{1,0:T(8,128)(2,1)} %q_ref.1, bf16[512,256]{1,0:T(8,128)(2,1)} %k_ref.1, bf16[512,256]{1,0:T(8,128)(2,1)} %v_ref.1, f32[2,8,128]{2,1,0:T(8,128)} %pad.4.f_ref, bf16[512,256]{1,0:T(8,128)(2,1)} %res_ref.1, bf16[2048,256]{1,0:T(8,128)(2,1)} %ow_ref.1, f32[1,128]{1,0:T(1,128)} %bitcast.8, ...), custom_call_target="tpu_custom_call" | custom-call | flops 40000000000 | bytes 100000000 | tf_op jit(solution)/shard_map/layer/pallas_call | solution.py:489
  214.6 1.7 copy.14

commit v3 on v2

--- a/solution.py
+++ b/solution.py
@@ -42,7 +42,7 @@
         return t + 1 - 2 * lax.rem(t, 2)
 
 
-def row_gather(row, buf, send, recv):
+def row_gather(row, buf, send, recv, between=lambda: None):
     half = buf.shape[1] // 2
     t, left, right, opp = row.t, row.left, row.right, row.opp
     other = Row.other
@@ -68,6 +68,7 @@
     go(buf.at[opp, first], 7, to_other)
     arrived(buf.at[opp, second], recv.at[5], to_right)
     go(buf.at[opp, second], 8, to_other)
+    between()
     arrived(buf.at[other(t)], recv.at[2], to_other)
     arrived(buf.at[other(left)], recv.at[4], to_other)
     arrived(buf.at[other(right)], recv.at[6], to_other)
@@ -120,6 +121,11 @@
     pair,
     total,
     landed,
+    xbuf,
+    xf,
+    send_x,
+    recv_x,
+    send_d,
     own_sem,
     send_w,
     recv_w,
@@ -156,59 +162,99 @@
     def hello(device):
         pl.semaphore_signal(barrier, inc=1, device_id=device, device_id_type=MESH)
 
-    for peer in (left, right, opp, other(t)):
-        hello({"tp": peer})
     hello(to_pair)
 
     @pl.loop(0, n_sp)
     def _(r):
         @pl.when(r != s)
         def _():
-            hello({"sp": r, "tp": t})
-
-        @pl.when(jnp.logical_or(r != s, t != source))
-        def _():
-            hello({"sp": r, "tp": source})
-
-    own = jnp.logical_or(row_of(2 * t) == s, row_of(2 * t + 1) == s)
-    pl.semaphore_wait(barrier, 5 + n_sp - 1 + 2 * n_tp - own.astype(jnp.int32))
-
-    def pieces(u, hi, keys):
-        there = lax.rem(t + u, n_tp)
-        rows, cols = pl.ds(there * sub, sub), pl.ds(hi * HEAD, HEAD)
-        if keys:
-            return there, (
-                (k_ref.at[rows, cols], kv.at[s, there, 0], 2, recv_a.at[s]),
-                (v_ref.at[rows, cols], kv.at[s, there, 1], 3, recv_a.at[s]),
-            )
-        return there, (
-            (q_ref.at[rows, cols], qbuf.at[s], 0, recv_a.at[n_sp]),
-            (f_ref.at[hi], fbuf.at[s], 1, recv_a.at[n_sp + 1]),
-        )
-
-    def each_piece(act, start, keys):
+            hello({"sp": r})
+
+    @pl.loop(0, n_tp)
+    def _(peer):
+        @pl.when(peer != t)
+        def _():
+            hello({"tp": peer})
+
+    pl.semaphore_wait(barrier, n_sp + n_tp - 1)
+    own = t == source
+    whole = pl.ds(0, sub)
+
+    def scatter(which):
         @pl.loop(0, n_tp)
-        def _(u):
+        def _(i):
+            there = lax.rem(t - s - i + n_sp + n_tp, n_tp)
+            rows = pl.ds(there * sub, sub)
+            cols = pl.ds(pl.multiple_of(lax.rem(my_head, 2) * HEAD, HEAD), HEAD)
+            for at in which:
+                ref = (k_ref, v_ref, q_ref)[at]
+                sem = recv_x.at[t, at]
+
+                @pl.when(there != t)
+                def _():
+                    remote(ref.at[rows], xbuf.at[t, at], send_x.at[at], sem, {"tp": there}).start()
+
+                @pl.when(there == t)
+                def _():
+                    pltpu.make_async_copy(ref.at[rows], xbuf.at[t, at], sem).start()
+
+                place = (kv.at[s, there, 0], kv.at[s, there, 1], qbuf.at[s])[at]
+                sem_a = recv_a.at[n_sp] if at == 2 else recv_a.at[s]
+
+                @pl.when(jnp.logical_and(own, there != t))
+                def _():
+                    remote(ref.at[rows, cols], place, send_d.at[at], sem_a, {"tp": there}).start()
+
+                @pl.when(jnp.logical_and(own, there == t))
+                def _():
+                    pltpu.make_async_copy(ref.at[rows, cols], place, sem_a).start()
+
+            if 2 in which:
+                mine = f_ref.at[lax.rem(my_head, 2)]
+
+                @pl.when(there != t)
+                def _():
+                    remote(f_ref, xf.at[t], send_x.at[3], recv_x.at[t, 3], {"tp": there}).start()
+
+                @pl.when(there == t)
+                def _():
+                    pltpu.make_async_copy(f_ref, xf.at[t], recv_x.at[t, 3]).start()
+
+                @pl.when(jnp.logical_and(own, there != t))
+                def _():
+                    remote(mine, fbuf.at[s], send_d.at[3], recv_a.at[n_sp + 1], {"tp": there}).start()
+
+                @pl.when(jnp.logical_and(own, there == t))
+                def _():
+                    pltpu.make_async_copy(mine, fbuf.at[s], recv_a.at[n_sp + 1]).start()
+
+    def deliver(which):
+        @pl.loop(0, n_tp)
+        def _(i):
+            src = lax.rem(t + s + i, n_tp)
+            if 2 in which:
+                arrived(xbuf.at[src, 2], recv_x.at[src, 2], {"tp": other(t)})
+                arrived(xf.at[src], recv_x.at[src, 3], {"tp": other(t)})
+            else:
+                arrived(xbuf.at[src, 0], recv_x.at[src, 0], {"tp": other(t)})
+                arrived(xbuf.at[src, 1], recv_x.at[src, 1], {"tp": other(t)})
             for hi in range(2):
-                r = row_of(2 * t + hi)
-                there, list_of = pieces(u, hi, keys)
-                mine = jnp.logical_and(r == s, there == t)
-
-                @pl.when(jnp.logical_not(mine))
-                def _():
-                    for src, dst, i, sem in list_of:
-                        act(remote(src, dst, send_a.at[hi, u, i], sem, {"sp": r, "tp": there}))
-
-                if start:
-
-                    @pl.when(mine)
-                    def _():
-                        for src, dst, _, sem in list_of:
-                            pltpu.make_async_copy(src, dst, sem).start()
+                r = row_of(2 * src + hi)
+                cols = pl.ds(hi * HEAD, HEAD)
+
+                @pl.when(r != s)
+                def _():
+                    for at in which:
+                        place = (kv.at[s, t, 0], kv.at[s, t, 1], qbuf.at[s])[at]
+                        sem_a = recv_a.at[n_sp] if at == 2 else recv_a.at[s]
+                        remote(xbuf.at[src, at, whole, cols], place, send_a.at[at], sem_a, {"sp": r}).start()
+                    if 2 in which:
+                        remote(xf.at[src, hi], fbuf.at[s], send_a.at[3], recv_a.at[n_sp + 1], {"sp": r}).start()
 
     third = w_ref.shape[0] // 3
-    ringed = pl.ds(pl.multiple_of(parity * third, 16), 2 * third)
-    shared = pl.ds(pl.multiple_of(parity * 2 * third, 16), third)
+    on_ring = w_ref.shape[0] // 32 * 16 + 16
+    ringed = pl.ds(pl.multiple_of(parity * (3 * third - on_ring), 16), on_ring)
+    shared = pl.ds(pl.multiple_of(parity * on_ring, 16), 3 * third - on_ring)
     half_way = n_sp // 2
 
     def chunk(d):
@@ -242,19 +288,20 @@
 
     own_copy = pltpu.make_async_copy(w_ref, wbuf.at[s], own_sem)
     own_copy.start()
-    each_piece(lambda c: c.start(), True, True)
-    pass_on(0, w_ref.at[ringed], s, to_next, 0)
-    pass_on(0, w_ref.at[ringed], s, to_last, 1)
-    each_piece(lambda c: c.start(), True, False)
+    scatter((0, 1))
+    scatter((2,))
+    deliver((0, 1))
+    deliver((2,))
 
     to_left, to_right, to_other = {"tp": left}, {"tp": right}, {"tp": other(t)}
 
-    def at_step(j):
-        d = (j + 1) // 2
-        return lax.rem(s + n_sp + jnp.where(lax.rem(j, 2) == 1, d, -d), n_sp)
+    per_turn = n_sp // n_tp
+
+    def at_step(owner, j):
+        return lax.rem(source - owner - j // per_turn + 2 * n_tp, n_tp) + n_tp * lax.rem(j, per_turn)
 
     def stage_one(j):
-        b = at_step(j)
+        b = at_step(t, j)
         arrived(kv.at[b, t], recv_a.at[b], to_other)
         piece = kv.at[b, t]
         remote(piece, piece, send_b.at[0], recv_b.at[0, b], to_right).start()
@@ -262,24 +309,23 @@
         remote(piece, piece, send_b.at[2], recv_c.at[0], to_other).start()
 
     def stage_two(j):
-        b = at_step(j)
+        b = at_step(left, j)
         arrived(kv.at[b, left], recv_b.at[0, b], to_left)
-        piece, part = kv.at[b, left], kv.at[b, left, 0]
-        remote(part, part, send_b.at[3], recv_b.at[2, b], to_right).start()
+        piece, half = kv.at[b, left], kv.at[b, left, 0]
+        remote(half, half, send_b.at[3], recv_b.at[2, b], to_right).start()
         remote(piece, piece, send_c.at[0], recv_c.at[1], to_other).start()
+        b = at_step(right, j)
         arrived(kv.at[b, right], recv_b.at[1, b], to_right)
-        piece, part = kv.at[b, right], kv.at[b, right, 1]
-        remote(part, part, send_b.at[4], recv_b.at[3, b], to_left).start()
+        piece, half = kv.at[b, right], kv.at[b, right, 1]
+        remote(half, half, send_b.at[4], recv_b.at[3, b], to_left).start()
         remote(piece, piece, send_c.at[1], recv_c.at[2], to_other).start()
 
     def stage_three(j):
-        b = at_step(j)
-        arrived(kv.at[b, opp, 0], recv_b.at[2, b], to_left)
-        part = kv.at[b, opp, 0]
-        remote(part, part, send_c.at[2], recv_c.at[3], to_other).start()
-        arrived(kv.at[b, opp, 1], recv_b.at[3, b], to_right)
-        part = kv.at[b, opp, 1]
-        remote(part, part, send_c.at[3], recv_c.at[4], to_other).start()
+        b = at_step(opp, j)
+        for i, (way, device) in enumerate(((2, to_left), (3, to_right))):
+            half = kv.at[b, opp, i]
+            arrived(half, recv_b.at[way, b], device)
+            remote(half, half, send_c.at[2 + i], recv_c.at[3 + i], to_other).start()
 
     lag = 2
 
@@ -297,9 +343,16 @@
         def _():
             stage_three(j - 2 * lag)
 
-        @pl.when(lax.rem(j, 4) == 3)
-        def _():
-            tick(j // 4 + 1)
+        @pl.when(lax.rem(j, 8) == 0)
+        def _():
+            @pl.when(j == 0)
+            def _():
+                pass_on(0, w_ref.at[ringed], s, to_next, 0)
+                pass_on(0, w_ref.at[ringed], s, to_last, 1)
+
+            @pl.when(j > 0)
+            def _():
+                tick(j // 8)
 
     arrived(kv.at[:, other(t)], recv_c.at[0], to_other)
     arrived(kv.at[:, other(left)], recv_c.at[1], to_other)
@@ -316,6 +369,7 @@
         rows = kv[b, :, 0].reshape(width, HEAD).astype(jnp.float32)
         kn[b] = normed(rows, kg_ref[...]).astype(jnp.bfloat16)
 
+    tick(3)
     group = 4
     tall, wide = group * sub, group * width
     factor = LOG2E / math.sqrt(HEAD)
@@ -330,7 +384,12 @@
 
     @pl.loop(0, n_sp // group)
     def _(step):
-        i = n_sp // group - 1 - step
+        i = lax.rem(s + step, n_sp // group)
+
+        @pl.when(step == 2)
+        def _():
+            tick(4)
+
         q = qbuf[pl.ds(i * group, group)].reshape(tall, HEAD).astype(jnp.float32)
         q = normed(q, qg_ref[...]).astype(jnp.bfloat16)
         base = fbuf[i * group, 0:1, 0:1]
@@ -374,7 +433,7 @@
             def _():
                 att[t, :, cols] = obuf[r]
 
-    tick(6)
+    tick(5)
 
     def o_wait(r):
         @pl.when(r != s)
@@ -382,10 +441,10 @@
             left_over(obuf.at[r], send_o.at[r], {"sp": r, "tp": t})
 
     pl.loop(0, n_sp)(o_wait)
+    tick(6)
     arrived(att.at[t, :, pl.ds(0, (n_sp - 1) * HEAD)], recv_o, to_other)
 
-    tick(7)
-    row_gather(row, att, send_g.at[0], recv_g.at[0])
+    row_gather(row, att, send_g.at[0], recv_g.at[0], lambda: tick(7))
     tick(8)
     total_rows = n_tp * sub
     span = 256
@@ -457,8 +516,18 @@
         left_over(part.at[k, 1 - core], send_p.at[k], to_other)
     for k in range(3):
         left_over(total.at[k], send_r.at[k], {"tp": chips[k]})
-    each_piece(lambda c: c.wait_send(), False, True)
-    each_piece(lambda c: c.wait_send(), False, False)
+    for at, ref in enumerate((k_ref, v_ref, q_ref)):
+        left_over(ref.at[pl.ds(0, (n_tp - 1) * sub)], send_x.at[at], to_other)
+        left_over(qbuf.at[pl.ds(0, n_sp - 1)], send_a.at[at], to_other)
+    left_over(xf.at[pl.ds(0, n_tp - 1)], send_x.at[3], to_other)
+    left_over(fbuf.at[pl.ds(0, n_sp - 1)], send_a.at[3], to_other)
+
+    @pl.when(own)
+    def _():
+        for at in range(3):
+            left_over(qbuf.at[pl.ds(0, n_tp - 1)], send_d.at[at], to_other)
+        left_over(fbuf.at[pl.ds(0, n_tp - 1)], send_d.at[3], to_other)
+
     left_over(kv.at[:, t], send_b.at[0], to_right)
     left_over(kv.at[:, t], send_b.at[1], to_left)
     left_over(kv.at[:, t], send_b.at[2], to_other)
@@ -499,7 +568,7 @@
             pltpu.VMEM((n_sp, sub, HEAD), bf),
             pltpu.VMEM((n_tp, sub, width), bf),
             pltpu.VMEM((n_tp, rows, cols), bf),
-            dma((2, n_tp, 4)),
+            dma((4,)),
             dma((n_sp + 2,)),
             dma((5,)),
             dma((4, n_sp)),
@@ -516,6 +585,11 @@
             pltpu.VMEM((4, rows, cols), bf),
             pltpu.VMEM((3, rows, cols), bf),
             pltpu.VMEM((3, rows, cols), bf),
+            pltpu.VMEM((n_tp, 3, sub, cols), bf),
+            pltpu.VMEM((n_tp, 2, 8, HEAD), jnp.float32),
+            dma((4,)),
+            dma((n_tp, 4)),
+            dma((4,)),
             dma,
             dma((2, n_sp // 2)),
             dma((2, n_sp // 2)),

time: 217 us -> 188 us (0.87)
  Pallas kernels: 211 us -> 183 us
    pallas_call x1, Pallas kernels: 211 us -> 183 us  [local(): pl.pallas_call(functools.partial(layer_kernel, n_sp, n_tp), out_shape=jax...]
where the time goes in v3:
time: 188 us
  Pallas kernels  183 us (97%)
  local copies, waits for them, and re-layouts  2.97 us (2%)
  other arithmetic  1.91 us (1%)
    pallas_call x1, Pallas kernels, local(): pl.pallas_call(functools.partial(layer_kernel, n_sp, n_tp), out_shape=jax...  183 us

profile of v3, /device:TPU:33, one launch (start us, length us, event | category | flops | bytes accessed | tf_op | source)
XLA Modules:
  0.0 187.9 jit_solution(3222369900801397624)
XLA Ops:
  0.0 0.7 reshape.12
  0.7 0.6 pad.4.f_ref
  1.3 1.9 %maximum_bitcast_fusion.w_ref = bf16[2064,128]{1,0:T(8,128)(2,1)} fusion(bf16[128,688]{0,1:T(8,128)(2,1)} %param.23, bf16[128,688]{0,1:T(8,128)(2,1)} %param.22, bf16[128,688]{0,1:T(8,128)(2,1)} %param.21), kind=kLoop, calls=%fused_computation | loop fusion | flops 1585152 | bytes 1056768 | tf_op jit(solution)/shard_map/transpose | solution.py:553
  3.2 183.0 %layer.1 = bf16[512,256]{1,0:T(8,128)(2,1)} custom-call(bf16[512,256]{1,0:T(8,128)(2,1)} %q_ref.1, bf16[512,256]{1,0:T(8,128)(2,1)} %k_ref.1, bf16[512,256]{1,0:T(8,128)(2,1)} %v_ref.1, f32[2,8,128]{2,1,0:T(8,128)} %pad.4.f_ref, bf16[512,256]{1,0:T(8,128)(2,1)} %res_ref.1, bf16[2048,256]{1,0:T(8,128)(2,1)} %ow_ref.1, f32[1,128]{1,0:T(1,128)} %bitcast.8, ...), custom_call_target="tpu_custom_call" | custom-call | flops 40000000000 | bytes 100000000 | tf_op jit(solution)/shard_map/layer/pallas_call | solution.py:558
  186.2 1.7 copy.14

commit v4 on v3

--- a/solution.py
+++ b/solution.py
@@ -288,9 +288,12 @@
 
     own_copy = pltpu.make_async_copy(w_ref, wbuf.at[s], own_sem)
     own_copy.start()
+    pass_on(0, w_ref.at[ringed], s, to_next, 0)
+    pass_on(0, w_ref.at[ringed], s, to_last, 1)
     scatter((0, 1))
     scatter((2,))
     deliver((0, 1))
+    tick(1)
     deliver((2,))
 
     to_left, to_right, to_other = {"tp": left}, {"tp": right}, {"tp": other(t)}
@@ -343,16 +346,9 @@
         def _():
             stage_three(j - 2 * lag)
 
-        @pl.when(lax.rem(j, 8) == 0)
-        def _():
-            @pl.when(j == 0)
-            def _():
-                pass_on(0, w_ref.at[ringed], s, to_next, 0)
-                pass_on(0, w_ref.at[ringed], s, to_last, 1)
-
-            @pl.when(j > 0)
-            def _():
-                tick(j // 8)
+        @pl.when(jnp.logical_and(j > 0, lax.rem(j, 8) == 0))
+        def _():
+            tick(j // 8 + 1)
 
     arrived(kv.at[:, other(t)], recv_c.at[0], to_other)
     arrived(kv.at[:, other(left)], recv_c.at[1], to_other)
@@ -369,7 +365,7 @@
         rows = kv[b, :, 0].reshape(width, HEAD).astype(jnp.float32)
         kn[b] = normed(rows, kg_ref[...]).astype(jnp.bfloat16)
 
-    tick(3)
+    tick(4)
     group = 4
     tall, wide = group * sub, group * width
     factor = LOG2E / math.sqrt(HEAD)
@@ -388,7 +384,7 @@
 
         @pl.when(step == 2)
         def _():
-            tick(4)
+            tick(5)
 
         q = qbuf[pl.ds(i * group, group)].reshape(tall, HEAD).astype(jnp.float32)
         q = normed(q, qg_ref[...]).astype(jnp.bfloat16)
@@ -433,8 +429,6 @@
             def _():
                 att[t, :, cols] = obuf[r]
 
-    tick(5)
-
     def o_wait(r):
         @pl.when(r != s)
         def _():
@@ -445,7 +439,6 @@
     arrived(att.at[t, :, pl.ds(0, (n_sp - 1) * HEAD)], recv_o, to_other)
 
     row_gather(row, att, send_g.at[0], recv_g.at[0], lambda: tick(7))
-    tick(8)
     total_rows = n_tp * sub
     span = 256
 
@@ -456,7 +449,7 @@
         product = jnp.dot(lhs, ow_ref[...], preferred_element_type=jnp.float32)
         mid[t, rows] = (res_ref[rows].astype(jnp.float32) + product).astype(jnp.bfloat16)
 
-    row_gather(row, mid, send_g.at[1], recv_g.at[1])
+    row_gather(row, mid, send_g.at[1], recv_g.at[1], lambda: tick(8))
     cols = mid.shape[2]
     rows = mid.shape[1]
     core = row.core

time: 188 us -> 181 us (0.963)
  Pallas kernels: 183 us -> 176 us
    pallas_call x1, Pallas kernels: 183 us -> 176 us  [local(): pl.pallas_call(functools.partial(layer_kernel, n_sp, n_tp), out_shape=jax...]
where the time goes in v4:
time: 181 us
  Pallas kernels  176 us (97%)
  local copies, waits for them, and re-layouts  2.97 us (2%)
  other arithmetic  1.91 us (1%)
    pallas_call x1, Pallas kernels, local(): pl.pallas_call(functools.partial(layer_kernel, n_sp, n_tp), out_shape=jax...  176 us

profile of v4, /device:TPU:33, one launch (start us, length us, event | category | flops | bytes accessed | tf_op | source)
XLA Modules:
  0.0 181.2 jit_solution(5464140323241269371)
XLA Ops:
  0.0 0.7 reshape.12
  0.7 0.6 pad.4.f_ref
  1.3 1.9 %maximum_bitcast_fusion.w_ref = bf16[2064,128]{1,0:T(8,128)(2,1)} fusion(bf16[128,688]{0,1:T(8,128)(2,1)} %param.23, bf16[128,688]{0,1:T(8,128)(2,1)} %param.22, bf16[128,688]{0,1:T(8,128)(2,1)} %param.21), kind=kLoop, calls=%fused_computation | loop fusion | flops 1585152 | bytes 1056768 | tf_op jit(solution)/shard_map/transpose | solution.py:546
  3.2 176.3 %layer.1 = bf16[512,256]{1,0:T(8,128)(2,1)} custom-call(bf16[512,256]{1,0:T(8,128)(2,1)} %q_ref.1, bf16[512,256]{1,0:T(8,128)(2,1)} %k_ref.1, bf16[512,256]{1,0:T(8,128)(2,1)} %v_ref.1, f32[2,8,128]{2,1,0:T(8,128)} %pad.4.f_ref, bf16[512,256]{1,0:T(8,128)(2,1)} %res_ref.1, bf16[2048,256]{1,0:T(8,128)(2,1)} %ow_ref.1, f32[1,128]{1,0:T(1,128)} %bitcast.8, ...), custom_call_target="tpu_custom_call" | custom-call | flops 40000000000 | bytes 100000000 | tf_op jit(solution)/shard_map/layer/pallas_call | solution.py:551
  179.5 1.7 copy.14
